TPU v7x, 256 devices: a 4x2x16 block of a 4x16x16 slice. The times are simulated.
256 devices in a mesh: grp: 2 (over y), sp: 32 (over z, core), tp: 4 (over x).
Axes of the slice: x: 4, y: 2, z: 16, core: 2. Of those that a mesh axis runs over, the one named last changes fastest.
The devices are a block of a 4x16x16 slice.
Arguments:
- ssm_input: bfloat16 [8192, 1024], P(('grp', 'sp'), 'tp'), parts along dimension 0, may hold values from -6 to 6
- residual_in: bfloat16 [8192, 2048], P(('grp', 'sp')), parts along dimension 0, may hold values from -4 to 4
- log_step: float32 [64], P('tp'), may hold values from -6.91 to -2.3
- decay_real: float32 [64, 64], P('tp'), may hold values from -34 to 0, as said below
- freq: float32 [64, 64], P('tp'), may hold values from 0.5 to 8
- in_real: float32 [64, 64, 16], P('tp'), may hold values from -1 to 1
- in_imag: float32 [64, 64, 16], P('tp'), may hold values from -1 to 1
- out_real: float32 [64, 16, 64], P('tp'), may hold values from -0.5 to 0.5
- out_imag: float32 [64, 16, 64], P('tp'), may hold values from -0.5 to 0.5
- skip: float32 [1024], P('tp'), may hold values from -3 to 3
- w_glu: bfloat16 [1024, 1024], replicated, may hold values from -0.1875 to 0.1875
- b_glu: float32 [1024], replicated, may hold values from -3 to 3
- w_branch: bfloat16 [1024, 2048], replicated, may hold values from -0.1875 to 0.1875
- norm_gain: float32 [2048], replicated, may hold values from 0.1 to 1.9
- w_gate: bfloat16 [2048, 5632], P('sp', 'tp'), may hold values from -0.125 to 0.125
- w_up: bfloat16 [2048, 5632], P('sp', 'tp'), may hold values from -0.125 to 0.125
- w_down: bfloat16 [5632, 2048], P('tp', 'sp'), may hold values from -0.078125 to 0.078125
Outputs:
- mixed: bfloat16 [8192, 2048], P(('grp', 'sp', 'tp')), parts along dimension 0
There are 2 independent parts, one for each index of `grp`. A program takes and returns all parts, laid end to end along the dimension named above; an argument that names none is the same for every part. Nothing has to cross between parts.
Inputs may be any that keep to these rules, and one draw needn't show every extreme that they name: `decay_real`: negative in every entry.
All inputs are finite; a program needn't handle non-finite values.
Results may differ from a plain program's by a relative error of at most 0.015.
Values may be sent and summed in bfloat16 or wider, within the bound.
A program may use at most 128 MiB of HBM per device.

v0:
```python
import math
import jax
import jax.numpy as jnp
from jax import lax
from jax.sharding import Mesh
from jax.sharding import PartitionSpec as P

SP = ("sp_0", "sp_1")
GRP_SP = ("grp", "sp_0", "sp_1")
GRP_SP_TP = ("grp", "sp_0", "sp_1", "tp")
EPS = 1e-06


def sent_together(arrays, axis, dim, along):
    ends, at = ([], 0)
    for a in arrays[:-1]:
        at += a.shape[along]
        ends.append(at)
    both = jnp.concatenate(arrays, axis=along)
    return tuple(jnp.split(lax.all_gather(both, axis, axis=dim, tiled=True), ends, axis=along))


def neutral_like(shard, identity):
    return jax.tree.map(
        lambda a, e: jnp.broadcast_to(jnp.asarray(e, a.dtype), a.shape), shard, identity
    )


def all_in_one(shard, axis):
    leaves = jax.tree.leaves(shard)
    turns = sorted(range(len(leaves)), key=lambda k: -leaves[k].size)
    width = (1, *leaves[turns[0]].shape)[-1]
    lines = [
        jnp.pad(leaves[k].reshape(-1), (0, -leaves[k].size % width)).reshape(-1, width)
        for k in turns
    ]
    both, at, found = (lax.all_gather(jnp.concatenate(lines), axis), 0, {})
    for k, line in zip(turns, lines):
        piece = both[:, at : at + len(line)].reshape(len(both), -1)
        found[k] = piece[:, : leaves[k].size].reshape(-1, *leaves[k].shape)
        at += len(line)
    numbers = iter(range(len(leaves)))
    return jax.tree.map(lambda _: found[next(numbers)], shard)


def entering_2(shard, axes, combine, identity):
    before = start = neutral_like(shard, identity)
    so_far = shard
    for axis in reversed(axes):
        count, place = (lax.axis_size(axis), lax.axis_index(axis))
        pieces = all_in_one(so_far, axis)
        inside, so_far = (start, start)
        for k in range(count):
            passed = k < place
            so_far = combine(so_far, jax.tree.map(lambda part: part[k], pieces))
            inside = jax.tree.map(lambda new, old: jnp.where(passed, new, old), so_far, inside)
        before = combine(inside, before)
    return before


def sent_to_all(shard, axis):
    count = lax.axis_size(axis)
    return lax.all_to_all(
        jnp.broadcast_to(shard[None], (count, *shard.shape)), axis, 0, 0, tiled=True
    )


def in_order(pieces, dim):
    dims = list(pieces.shape[1:])
    dims[dim] *= pieces.shape[0]
    return jnp.moveaxis(pieces, 0, dim).reshape(dims)


def gather_directly(shard, axis, dim):
    pieces = sent_to_all(shard, axis)
    return in_order(pieces, dim)


def cut_along(shard, dim, count):
    dims = shard.shape
    pieces = shard.reshape(*dims[:dim], count, dims[dim] // count, *dims[dim + 1 :])
    return jnp.moveaxis(pieces, dim, 0)


def summed_on_arrival(shard, axis, dim):
    pieces = cut_along(shard, dim, lax.axis_size(axis))
    arrived = lax.all_to_all(pieces, axis, split_axis=0, concat_axis=0, tiled=True)
    return arrived.astype(jnp.float32).sum(axis=0)


def discretize(log_step, decay_real, freq, in_real, in_imag):
    step_size = jnp.exp(log_step)[:, None]
    magnitude = jnp.exp(decay_real * step_size)
    abar_re = magnitude * jnp.cos(freq * step_size)
    abar_im = magnitude * jnp.sin(freq * step_size)
    denominator = decay_real * decay_real + freq * freq
    less_re = abar_re - 1.0
    hold_re = ((less_re * decay_real + abar_im * freq) / denominator)[..., None]
    hold_im = ((abar_im * decay_real - less_re * freq) / denominator)[..., None]
    bbar_re = hold_re * in_real - hold_im * in_imag
    bbar_im = hold_re * in_imag + hold_im * in_real
    return (step_size, abar_re, abar_im, bbar_re, bbar_im)


def powers(decay_real, freq, step_size, length):
    steps_up = (jnp.arange(length, dtype=jnp.int32) + 1).astype(jnp.float32)[:, None, None]
    magnitude = jnp.exp((decay_real * step_size)[None] * steps_up)
    phase = (freq * step_size)[None] * steps_up
    return (magnitude * jnp.cos(phase), magnitude * jnp.sin(phase))


def compose(earlier, later):
    a1r, a1i, b1r, b1i = earlier
    a2r, a2i, b2r, b2i = later
    return (
        a2r * a1r - a2i * a1i,
        a2r * a1i + a2i * a1r,
        a2r * b1r - a2i * b1i + b2r,
        a2r * b1i + a2i * b1r + b2i,
    )


def local_states(inputs, decay_real, freq, step_size, bbar_re, bbar_im):
    highest = lax.Precision.DEFAULT
    tok_rows, group_count, unused = inputs.shape
    lanes = group_count * decay_real.shape[1]
    drive_re = jnp.einsum("lgm,gpm->lgp", inputs, bbar_re, precision=highest).reshape(
        tok_rows, lanes
    )
    drive_im = jnp.einsum("lgm,gpm->lgp", inputs, bbar_im, precision=highest).reshape(
        tok_rows, lanes
    )
    span = math.gcd(tok_rows, 16)
    spans = tok_rows // span
    rate = (decay_real * step_size).reshape(lanes)
    turn = (freq * step_size).reshape(lanes)
    later = jnp.arange(span, dtype=jnp.int32)[:, None]
    earlier = jnp.arange(span, dtype=jnp.int32)[None, :]
    lag = (later - earlier).astype(jnp.float32)
    causal = (later >= earlier)[..., None]
    lag_pos = jnp.maximum(lag, 0.0)[..., None]
    table_mag = jnp.exp(rate[None, None] * lag_pos)
    table_re = jnp.where(causal, table_mag * jnp.cos(turn[None, None] * lag_pos), 0.0)
    table_im = jnp.where(causal, table_mag * jnp.sin(turn[None, None] * lag_pos), 0.0)
    block_re = drive_re.reshape(spans, 1, span, lanes)
    block_im = drive_im.reshape(spans, 1, span, lanes)
    inner_re = jnp.sum(table_re[None] * block_re - table_im[None] * block_im, axis=2)
    inner_im = jnp.sum(table_re[None] * block_im + table_im[None] * block_re, axis=2)
    steps_up = (jnp.arange(span, dtype=jnp.int32) + 1).astype(jnp.float32)[:, None]
    pow_mag = jnp.exp(rate[None] * steps_up)
    pow_re = pow_mag * jnp.cos(turn[None] * steps_up)
    pow_im = pow_mag * jnp.sin(turn[None] * steps_up)
    span_re = pow_re[-1]
    span_im = pow_im[-1]

    def carry_step(entering, ends):
        next_re = span_re * entering[0] - span_im * entering[1] + ends[0]
        next_im = span_re * entering[1] + span_im * entering[0] + ends[1]
        return ((next_re, next_im), entering)

    zeros = jnp.zeros((lanes,), jnp.float32)
    unused_carry, entering = lax.scan(
        carry_step, (zeros, zeros), (inner_re[:, -1], inner_im[:, -1])
    )
    state_re = inner_re + pow_re[None] * entering[0][:, None] - pow_im[None] * entering[1][:, None]
    state_im = inner_im + pow_re[None] * entering[1][:, None] + pow_im[None] * entering[0][:, None]
    shape = (tok_rows, group_count, decay_real.shape[1])
    return (state_re.reshape(shape), state_im.reshape(shape))


def readout(state_re, state_im, out_real, out_imag, skip_mat, inputs):
    highest = lax.Precision.DEFAULT
    values = (
        jnp.einsum("lgp,gmp->lgm", state_re, out_real, precision=highest)
        - jnp.einsum("lgp,gmp->lgm", state_im, out_imag, precision=highest)
        + skip_mat[None] * inputs
    )
    values = jax.nn.gelu(values)
    return values.reshape(values.shape[0], -1).astype(jnp.bfloat16)


def row_norm(stream, norm_gain):
    scale_rows = lax.rsqrt(jnp.mean(stream * stream, axis=-1, keepdims=True) + EPS)
    return (stream * scale_rows * norm_gain).astype(jnp.bfloat16)


def per_device(
    ssm_input,
    residual_in,
    log_step,
    decay_real,
    freq,
    in_real,
    in_imag,
    out_real,
    out_imag,
    skip,
    w_glu,
    b_glu,
    w_branch,
    norm_gain,
    w_gate,
    w_up,
    w_down,
):
    tok_rows, width_local = ssm_input.shape
    group_count = log_step.shape[0]
    group_size = in_real.shape[2]
    tp_count = lax.axis_size("tp")
    tp_index = lax.axis_index("tp")
    own_rows = tok_rows // tp_count
    gate_whole, up_whole = sent_together((w_gate, w_up), SP, 0, 1)
    step_size, abar_re, abar_im, bbar_re, bbar_im = discretize(
        log_step, decay_real, freq, in_real, in_imag
    )
    pow_re, pow_im = powers(decay_real, freq, step_size, tok_rows)
    inputs = ssm_input.astype(jnp.float32).reshape(tok_rows, group_count, group_size)
    local_re, local_im = local_states(inputs, decay_real, freq, step_size, bbar_re, bbar_im)
    identity = (
        jnp.ones_like(abar_re),
        jnp.zeros_like(abar_re),
        jnp.zeros_like(abar_re),
        jnp.zeros_like(abar_re),
    )
    carried = entering_2(
        (pow_re[-1], pow_im[-1], local_re[-1], local_im[-1]), SP, compose, identity
    )
    state_re = local_re + pow_re * carried[2][None] - pow_im * carried[3][None]
    state_im = local_im + pow_re * carried[3][None] + pow_im * carried[2][None]
    mixer_out = readout(
        state_re, state_im, out_real, out_imag, skip.reshape(group_count, group_size), inputs
    )
    mixer_rows = lax.all_to_all(mixer_out, "tp", split_axis=0, concat_axis=1, tiled=True)
    glu_pre = jnp.dot(mixer_rows, w_glu, preferred_element_type=jnp.float32) + b_glu
    gated = (mixer_rows.astype(jnp.float32) * jax.nn.sigmoid(glu_pre)).astype(jnp.bfloat16)
    residual_own = lax.dynamic_slice_in_dim(residual_in, tp_index * own_rows, own_rows, 0)
    stream = residual_own.astype(jnp.float32) + jnp.dot(
        gated, w_branch, preferred_element_type=jnp.float32
    )
    normed = row_norm(stream, norm_gain)
    normed_all = gather_directly(normed, "tp", 0)
    gate_sum = jnp.dot(normed_all, gate_whole, preferred_element_type=jnp.float32)
    up_sum = jnp.dot(normed_all, up_whole, preferred_element_type=jnp.float32)
    hidden = (jax.nn.silu(gate_sum) * up_sum).astype(jnp.bfloat16)
    down_whole = lax.all_gather(w_down, SP, axis=1, tiled=True)
    summed = summed_on_arrival(
        jnp.dot(hidden, down_whole, preferred_element_type=jnp.float32).astype(jnp.bfloat16),
        "tp",
        0,
    )
    return (stream + summed).astype(jnp.bfloat16)


def solution(mesh):
    torus = Mesh(
        mesh.devices.reshape(mesh.shape["grp"], 16, 2, mesh.shape["tp"]),
        ("grp", "sp_0", "sp_1", "tp"),
    )
    in_specs = (
        P(GRP_SP, "tp"),
        P(GRP_SP, None),
        P("tp"),
        P("tp", None),
        P("tp", None),
        P("tp", None, None),
        P("tp", None, None),
        P("tp", None, None),
        P("tp", None, None),
        P("tp"),
        P(),
        P(),
        P(),
        P(),
        P(SP, "tp"),
        P(SP, "tp"),
        P("tp", SP),
    )
    out_specs = P(GRP_SP_TP, None)
    return jax.shard_map(
        per_device, mesh=torus, in_specs=in_specs, out_specs=out_specs, check_vma=False
    )
```

profile of v0, /device:TPU:33, one launch (start us, length us, event | category | flops | bytes accessed | tf_op | source)
XLA Modules:
  0.0 209.0 jit_solution(3152876637672829027)
XLA Ops:
  6.6 1.9 pad_maximum_fusion
  8.6 0.7 all-gather.7.cloned.1.call-update
  9.4 0.7 exp.36
  10.0 0.8 fusion.68
  11.0 0.9 copy.43
  12.0 5.8 %fusion.19 = (f32[16,16,1024]{2,1,0:T(8,128)}, f32[16,16,1024]{2,1,0:T(8,128)}) fusion(f32[1024]{0:T(1024)S(1)} %mul.861, f32[16,16]{1,0:T(8,128)S(1)} %convert_maximum_fusion, f32[1024]{0:T(1024)S(1)} %mul.856, pred[16,16]{1,0:T(8,128)(4,1)S(1)} %iota_compare_fusion), kind=kLoop, calls=%fused_computation.33 | loop fusion | flops 1572864 | bytes 2106624 | tf_op jit(solution)/shard_map/jit(_where)/select_n | solution.py:143
  17.8 2.0 convolution_bitcast_fusion.1
  19.8 2.0 convolution_bitcast_fusion
  21.8 1.5 copy.44
  23.4 1.1 mul.878
  24.5 1.5 copy.45
  26.1 1.1 mul.885
  27.2 6.3 %add_reduce_fusion = (f32[8,16,1024]{2,1,0:T(8,128)S(1)}, f32[8,16,1024]{2,1,0:T(8,128)S(1)}) fusion(f32[8,16,1024]{2,1,0:T(8,128)} %mul.885, f32[16,16,1024]{2,1,0:T(8,128)} %get-tuple-element.125, f32[8,16,1024]{2,1,0:T(8,128)} %mul.878, f32[16,16,1024]{2,1,0:T(8,128)} %get-tuple-element.124), kind=kLoop, calls=%fused_computation.6 | loop fusion | flops 16515072 | bytes 4194304 | tf_op jit(solution)/shard_map/reduce_sum | solution.py:148
  33.6 0.3 fusion.55
  34.0 12.5 %while.17 = (s32[]{:T(128)}, f32[1024]{0:T(1024)S(1)}, f32[1024]{0:T(1024)S(1)}, f32[8,1024]{1,0:T(8,128)S(1)}, f32[8,1024]{1,0:T(8,128)}, /*index=5*/f32[1024]{...) while((s32[]{:T(128)}, f32[1024]{0:T(1024)S(1)}, ...), condition=%wide.region_3.4_spmd.clone, body=%wide.region_2.3_spmd.clone.sunk | while | flops 10243 | bytes 90243 | solution.py:162
  34.0 0.1 dynamic_update_slice.11
  34.2 1.4 dynamic_update_slice.12
  35.6 0.1 dynamic_update_slice.11
  35.7 1.4 dynamic_update_slice.12
  37.2 0.1 dynamic_update_slice.11
  37.3 1.4 dynamic_update_slice.12
  38.7 0.1 dynamic_update_slice.11
  38.9 1.4 dynamic_update_slice.12
  40.4 1.4 dynamic_update_slice.12
  42.0 1.4 dynamic_update_slice.12
  43.5 1.4 dynamic_update_slice.12
  45.1 1.4 dynamic_update_slice.12
  46.5 1.9 multiply_add_fusion.1
  48.4 1.3 add.447
  49.8 2.3 %sub.173 = f32[128,16,64]{2,1,0:T(8,128)} reshape(f32[8,16,1024]{2,1,0:T(8,128)} %get-tuple-element.118) | data formatting | bytes 1048576 | tf_op jit(solution)/shard_map/sub | solution.py:165
  52.2 0.7 slice_bitcast_fusion.1
  52.9 3.9 %fusion.22 = (f32[128,16,64]{2,1,0:T(8,128)S(1)}, f32[128,16,64]{2,1,0:T(8,128)S(1)}) fusion(f32[16,64]{1,0:T(8,128)S(1)} %get-tuple-element.133, f32[128]{0:T(128)S(1)} %add_convert_fusion.1, f32[16,64]{1,0:T(8,128)S(1)} %get-tuple-element.132), kind=kLoop, calls=%fused_computation.36 | loop fusion | flops 524288 | bytes 1057280 | tf_op jit(solution)/shard_map/mul | solution.py:109
  56.8 22.0 %all-gather = f32[128,64]{1,0:T(8,128)S(1)} all-gather(f32[64,64]{1,0:T(8,128)S(1)} %pad_maximum_fusion.1), channel_id=2, replica_groups=mesh['grp'=2,'sp_0'=16,'sp_1'=2,'tp'=4] {'sp_1'}, dimensions={0}, use_global_device_ids=true | all-gather | bytes 49152 | tf_op jit(solution)/shard_map/all_gather | solution.py:37
  78.9 31.6 %all-gather.1 = f32[1024,64]{1,0:T(8,128)S(1)} all-gather(f32[64,64]{1,0:T(8,128)S(1)} %pad_maximum_fusion.2), channel_id=3, replica_groups=mesh['grp'=2,'sp_0'=16,'sp_1'=2,'tp'=4] {'sp_0'}, dimensions={0}, use_global_device_ids=true | all-gather | bytes 278528 | tf_op jit(solution)/shard_map/all_gather | solution.py:37
  110.6 6.7 %multiply_add_fusion = (bf16[128,16,64]{2,1,0:T(8,128)(2,1)S(1)}, bf16[128,16,64]{2,1,0:T(8,128)(2,1)S(1)}) fusion(f32[128,16,64]{2,1,0:T(8,128)S(1)} %add.447, f32[16,64]{1,0:T(8,128)S(1)} %add_bitcast_fusion, f32[16,64]{1,0:T(8,128)S(1)} %get-tuple-element.108, f32[16,64]{1,0:T(8,128)S(1)} %get-tuple-element.133, f32[128]{0:T(128)S(1)} %add_convert_fusion.1, ...), kind=kLoop, calls=%fused_computation.42 | loop fusion | flops 1835008 | bytes 1589760 | tf_op jit(solution)/shard_map/add | solution.py:229
  117.3 0.4 fusion.25
  117.7 1.3 fusion.44
  119.0 0.2 convert_element_type.64
  119.2 0.8 copy.48
  120.0 4.2 %all-to-all-start = ((bf16[4,32,256]{2,1,0:T(8,128)(2,1)}), bf16[4,32,256]{2,1,0:T(8,128)(2,1)S(1)}, u32[]{:S(2)}, u32[]{:S(2)}) async-start(bf16[4,32,256]{2,1,0:T(8,128)(2,1)} %copy.48), calls=%async_computation | async-start | bytes 131072 | tf_op jit(solution)/shard_map/all_to_all | solution.py:233
  124.2 4.5 %all-to-all-done = bf16[4,32,256]{2,1,0:T(8,128)(2,1)S(1)} async-done(((bf16[4,32,256]{2,1,0:T(8,128)(2,1)}), bf16[4,32,256]{2,1,0:T(8,128)(2,1)S(1)}, u32[]{:S(2)}, u32[]{:S(2)}) %all-to-all-start) | async-done | bytes 65568 | tf_op jit(solution)/shard_map/all_to_all | solution.py:233
  128.7 3.5 %multiply_reduce_fusion = (f32[32]{0:T(128)S(1)}, f32[32,2048]{1,0:T(8,128)S(1)}) fusion(bf16[1024,2048]{1,0:T(8,128)(2,1)} %param.31, bf16[32,1024]{1,0:T(8,128)(2,1)S(1)} %bitcast.174, bf16[1024,1024]{1,0:T(8,128)(2,1)S(1)} %copy-done, f32[1024]{0:T(1024)S(1)} %copy-done.3, bf16[128,2048]{1,0:T(8,128)(2,1)} %param.20, s32[]{:T(128)S(6)} %select_n.296), kind=kOutput, calls=%fused_computation.57 | convolution fusion | flops 201818080 | bytes 6819972 | tf_op jit(solution)/shard_map/dot_general | solution.py:237
  132.4 9.4 %all_to_all.26 = bf16[4,32,2048]{2,1,0:T(8,128)(2,1)S(1)} all-to-all(bf16[4,32,2048]{2,1,0:T(8,128)(2,1)S(1)} %broadcast_in_dim.32), channel_id=1, replica_groups=mesh['grp'=2,'sp_0'=16,'sp_1'=2,'tp'=4] {'tp'}, dimensions={0} | all-to-all | bytes 1048576 | tf_op jit(solution)/shard_map/all_to_all | solution.py:63
  141.8 4.6 %fusion.2 = f32[128,1408]{1,0:T(8,128)} fusion(bf16[128,2048]{1,0:T(8,128)(2,1)S(1)} %bitcast.167, bf16[2048,2816]{1,0:T(8,128)(2,1)} %all-gather.5.cloned.1.call-done), kind=kOutput, calls=%fused_computation.10 | convolution fusion | flops 738197504 | bytes 7012352 | tf_op jit(solution)/shard_map/dot_general | solution.py:242
  146.3 34.8 %all-gather.7.cloned.1.call-done = bf16[1408,2048]{0,1:T(8,128)(2,1)} async-done(((bf16[1408,64]{0,1:T(8,128)(2,1)}), bf16[1408,2048]{0,1:T(8,128)(2,1)}) %all-gather.7.cloned.1.call-update) | async-done | bytes 5767184 | tf_op jit(solution)/shard_map/all_gather | solution.py:245
  181.1 7.4 %convolution_convert_fusion = bf16[128,2048]{1,0:T(8,128)(2,1)S(1)} fusion(bf16[1408,2048]{0,1:T(8,128)(2,1)} %all-gather.7.cloned.1.call-done, bf16[128,2048]{1,0:T(8,128)(2,1)S(1)} %bitcast.168, bf16[2048,2816]{1,0:T(8,128)(2,1)} %all-gather.5.cloned.1.call-done, f32[128,1408]{1,0:T(8,128)} %fusion.2), kind=kOutput, calls=%fused_computation.14 | convolution fusion | flops 1477738496 | bytes 13303808 | tf_op jit(solution)/shard_map/dot_general | solution.py:247
  188.6 12.9 %all_to_all.27 = bf16[4,32,2048]{2,1,0:T(8,128)(2,1)S(1)} all-to-all(bf16[4,32,2048]{2,1,0:T(8,128)(2,1)S(1)} %bitcast.169), channel_id=1, replica_groups=mesh['grp'=2,'sp_0'=16,'sp_1'=2,'tp'=4] {'tp'}, dimensions={0} | all-to-all | bytes 1048576 | tf_op jit(solution)/shard_map/all_to_all | solution.py:87
  201.5 0.7 add_convert_fusion
  (71 shorter events, 1.5 us)
Async XLA Ops:
  6.5 122.1 %copy-start = (bf16[1024,1024]{1,0:T(8,128)(2,1)S(1)}, bf16[1024,1024]{1,0:T(8,128)(2,1)}, u32[]{:S(2)}) copy-start(bf16[1024,1024]{1,0:T(8,128)(2,1)} %param.29) | copy-start | bytes 6291460
  6.6 135.2 %all-gather.5.cloned.1.call-start = ((), (), s32[]{:S(2)}) async-start(), calls=%async_computation.3 | async-start | bytes 11894784 | tf_op jit(solution)/shard_map/all_gather | solution.py:20
  8.5 172.6 %all-gather.7.cloned.1.call-start = ((), (), s32[]{:S(2)}) async-start(), calls=%async_computation.4 | async-start | bytes 5947392 | tf_op jit(solution)/shard_map/all_gather | solution.py:245
  27.2 24.9 %copy-start.4 = (f32[256]{0:T(256)S(1)}, f32[256]{0:T(256)}, u32[]{:S(2)}) copy-start(f32[256]{0:T(256)} %param.28) | copy-start | bytes 3076
  46.5 70.8 %copy-start.1 = (f32[16,16,64]{2,1,0:T(8,128)S(1)}, f32[16,16,64]{2,1,0:T(8,128)}, u32[]{:S(2)}) copy-start(f32[16,16,64]{2,1,0:T(8,128)} %param.26) | copy-start | bytes 196612
  49.8 78.9 %copy-start.3 = (f32[1024]{0:T(1024)S(1)}, f32[1024]{0:T(1024)}, u32[]{:S(2)}) copy-start(f32[1024]{0:T(1024)} %param.30) | copy-start | bytes 12292
  110.6 21.7 %copy-start.2 = (f32[2048]{0:T(1024)S(1)}, f32[2048]{0:T(1024)}, u32[]{:S(2)}) copy-start(f32[2048]{0:T(1024)} %param.32) | copy-start | bytes 24580
  120.0 8.7 %all-to-all-start = ((bf16[4,32,256]{2,1,0:T(8,128)(2,1)}), bf16[4,32,256]{2,1,0:T(8,128)(2,1)S(1)}, u32[]{:S(2)}, u32[]{:S(2)}) async-start(bf16[4,32,256]{2,1,0:T(8,128)(2,1)} %copy.48), calls=%async_computation | async-start | bytes 131072 | tf_op jit(solution)/shard_map/all_to_all | solution.py:233
Sparse Core Ops, SparseCore 0:
  9.2 101.0 all-gather.4
  112.1 68.9 all-gather.6
where the time goes:
time: 210 us; the launch traced here: 209 us
  blocking collectives  75.9 us (36%)
  waiting for transfers between devices  40.1 us (19%)
  other arithmetic  28.9 us (14%)
  local copies, waits for them, and re-layouts  24.7 us (12%)
  matrix products  21.3 us (10%)
  between operations  13.7 us (7%)
  starting transfers between devices  4.27 us (2%)
    all_gather x2, blocking collectives, all_in_one(): both, at, found = (lax.all_gather(jnp.concatenate(lines), axis), 0, {})  53.6 us
    all_gather x1, waiting for transfers between devices, per_device(): down_whole = lax.all_gather(w_down, SP, axis=1, tiled=True)  34.8 us
    all_to_all x1, blocking collectives, summed_on_arrival(): lax.all_to_all(pieces, axis, split_axis=0, concat_axis=0, tiled=True)  12.9 us
    dynamic_update_slice x16, local copies, waits for them, and re-layouts, local_states(): lax.scan(carry_step, (zeros, zeros), (inner_re[:, -1], inner_im[:, -1]))  12.1 us
    all_to_all x1, blocking collectives, sent_to_all(): lax.all_to_all(jnp.broadcast_to(shard[None], (count, *shard.shape)), axis...  9.36 us
    dot_general x1, matrix products, per_device(): jnp.dot(hidden, down_whole, preferred_element_type=jnp.float32)  7.42 us
    add x1, other arithmetic, per_device(): state_im = local_im + pow_re * carried[3][None] + pow_im * carried[2][None]  6.71 us
    reduce_sum x1, other arithmetic, local_states(): jnp.sum(table_re[None] * block_im + table_im[None] * block_re, axis=2)  6.35 us
  transfers between devices with their start and end apart: 3, of which 2 were waited for; matrix products, arithmetic and copies ran while one was open for 31% of the time, Pallas kernels for 0%

commit v1 on v0

--- a/solution.py
+++ b/solution.py
@@ -242,7 +242,8 @@
     gate_sum = jnp.dot(normed_all, gate_whole, preferred_element_type=jnp.float32)
     up_sum = jnp.dot(normed_all, up_whole, preferred_element_type=jnp.float32)
     hidden = (jax.nn.silu(gate_sum) * up_sum).astype(jnp.bfloat16)
-    down_whole = lax.all_gather(w_down, SP, axis=1, tiled=True)
+    blocks = lax.all_gather(w_down, SP, axis=0, tiled=False)
+    down_whole = jnp.concatenate(blocks, axis=1)
     summed = summed_on_arrival(
         jnp.dot(hidden, down_whole, preferred_element_type=jnp.float32).astype(jnp.bfloat16),
         "tp",

time: 210 us -> 212 us (level)
  blocking collectives: 75.9 us -> 62.5 us
  local copies, waits for them, and re-layouts: 24.7 us -> 33.7 us
  waiting for transfers between devices: 40.1 us -> 44.5 us
  starting transfers between devices: 4.27 us -> 7.66 us
    all_gather x1, waiting for transfers between devices: 0.01 us -> 39.1 us  [sent_together(): lax.all_gather(both, axis, axis=dim, tiled=True)]
    all_gather x1, waiting for transfers between devices: 34.8 us -> 0.02 us  [per_device(): blocks = lax.all_gather(w_down, SP, axis=0, tiled=False)]
    all_to_all x1 -> x0, blocking collectives: 9.36 us -> none  [sent_to_all(): lax.all_to_all(jnp.broadcast_to(shard[None], (count, *shard.shape)), axis...]
    reshape x0 -> x1, local copies, waits for them, and re-layouts: none -> 4.45 us  [per_device(): down_whole = jnp.concatenate(blocks, axis=1)]
    all_gather x2, blocking collectives: 53.6 us -> 49.7 us  [all_in_one(): both, at, found = (lax.all_gather(jnp.concatenate(lines), axis), 0, {})]
    all_to_all x0 -> x1, starting transfers between devices: none -> 3.79 us  [sent_to_all(): lax.all_to_all(jnp.broadcast_to(shard[None], (count, *shard.shape)), axis...]
    unnamed x12 -> x13, local copies, waits for them, and re-layouts: 0.99 us -> 4.71 us
  transfers between devices with their start and end apart: 3 -> 4, of which waited for: 2 -> 2; matrix products, arithmetic and copies ran while one was open for 31% -> 33% of each run, Pallas kernels for 0% -> 0%
where the time goes in v1:
time: 212 us; the launch traced here: 210 us
  blocking collectives  62.5 us (29%)
  waiting for transfers between devices  44.5 us (21%)
  local copies, waits for them, and re-layouts  33.7 us (16%)
  other arithmetic  26.8 us (13%)
  matrix products  21.4 us (10%)
  between operations  13.7 us (6%)
  starting transfers between devices  7.66 us (4%)
    all_gather x2, blocking collectives, all_in_one(): both, at, found = (lax.all_gather(jnp.concatenate(lines), axis), 0, {})  49.7 us
    all_gather x1, waiting for transfers between devices, sent_together(): lax.all_gather(both, axis, axis=dim, tiled=True)  39.1 us
    all_to_all x1, blocking collectives, summed_on_arrival(): lax.all_to_all(pieces, axis, split_axis=0, concat_axis=0, tiled=True)  12.8 us
    dynamic_update_slice x16, local copies, waits for them, and re-layouts, local_states(): lax.scan(carry_step, (zeros, zeros), (inner_re[:, -1], inner_im[:, -1]))  12.1 us
    dot_general x1, matrix products, per_device(): jnp.dot(hidden, down_whole, preferred_element_type=jnp.float32)  7.42 us
    add x1, other arithmetic, per_device(): state_im = local_im + pow_re * carried[3][None] + pow_im * carried[2][None]  6.71 us
    reduce_sum x1, other arithmetic, local_states(): jnp.sum(table_re[None] * block_im + table_im[None] * block_re, axis=2)  6.2 us
    unnamed x13, local copies, waits for them, and re-layouts  4.71 us
  transfers between devices with their start and end apart: 4, of which 2 were waited for; matrix products, arithmetic and copies ran while one was open for 33% of the time, Pallas kernels for 0%

profile of v1, /device:TPU:33, one launch (start us, length us, event | category | flops | bytes accessed | tf_op | source)
XLA Modules:
  0.0 210.5 jit_solution(13554760460877968577)
XLA Ops:
  6.6 0.7 all-gather.8.cloned.1.call-update
  7.4 1.8 pad_maximum_fusion
  9.3 1.0 copy.53
  10.2 0.7 exp.36
  10.9 0.8 fusion.68
  11.7 2.0 convolution_bitcast_fusion
  13.8 1.5 copy.55
  15.3 1.1 mul.885
  16.6 2.1 convolution_bitcast_fusion.1
  18.6 1.5 copy.54
  20.2 1.1 mul.878
  21.3 0.3 fusion.55
  21.7 4.0 %fusion.19 = (f32[16,16,1024]{2,1,0:T(8,128)S(1)}, f32[16,16,1024]{2,1,0:T(8,128)S(1)}) fusion(f32[1024]{0:T(1024)S(1)} %mul.861, f32[16,16]{1,0:T(8,128)S(1)} %convert_maximum_fusion, f32[1024]{0:T(1024)S(1)} %mul.856, pred[16,16]{1,0:T(8,128)(4,1)S(1)} %iota_compare_fusion), kind=kLoop, calls=%fused_computation.33 | loop fusion | flops 1572864 | bytes 2106624 | tf_op jit(solution)/shard_map/jit(_where)/select_n | solution.py:143
  25.7 6.2 %add_reduce_fusion = (f32[8,16,1024]{2,1,0:T(8,128)S(1)}, f32[8,16,1024]{2,1,0:T(8,128)S(1)}) fusion(f32[8,16,1024]{2,1,0:T(8,128)} %mul.885, f32[16,16,1024]{2,1,0:T(8,128)S(1)} %get-tuple-element.125, f32[8,16,1024]{2,1,0:T(8,128)} %mul.878, f32[16,16,1024]{2,1,0:T(8,128)S(1)} %get-tuple-element.124), kind=kLoop, calls=%fused_computation.6 | loop fusion | flops 16515072 | bytes 4194304 | tf_op jit(solution)/shard_map/reduce_sum | solution.py:148
  32.0 12.5 %while.17 = (s32[]{:T(128)}, f32[1024]{0:T(1024)S(1)}, f32[1024]{0:T(1024)S(1)}, f32[8,1024]{1,0:T(8,128)S(1)}, f32[8,1024]{1,0:T(8,128)}, /*index=5*/f32[1024]{...) while((s32[]{:T(128)}, f32[1024]{0:T(1024)S(1)}, ...), condition=%wide.region_3.4_spmd.clone, body=%wide.region_2.3_spmd.clone.sunk | while | flops 10243 | bytes 90251 | solution.py:162
  32.2 1.4 dynamic_update_slice.12
  33.7 1.4 dynamic_update_slice.12
  35.3 1.4 dynamic_update_slice.12
  36.9 1.4 dynamic_update_slice.12
  38.3 0.1 dynamic_update_slice.11
  38.4 1.4 dynamic_update_slice.12
  40.0 1.4 dynamic_update_slice.12
  41.6 1.4 dynamic_update_slice.12
  43.1 1.4 dynamic_update_slice.12
  44.5 1.9 multiply_add_fusion.1
  46.4 1.3 add.447
  47.8 2.3 %sub.173 = f32[128,16,64]{2,1,0:T(8,128)} reshape(f32[8,16,1024]{2,1,0:T(8,128)} %get-tuple-element.118) | data formatting | bytes 1048576 | tf_op jit(solution)/shard_map/sub | solution.py:165
  50.2 0.7 slice_bitcast_fusion.1
  50.9 3.9 %fusion.22 = (f32[128,16,64]{2,1,0:T(8,128)S(1)}, f32[128,16,64]{2,1,0:T(8,128)S(1)}) fusion(f32[16,64]{1,0:T(8,128)S(1)} %get-tuple-element.133, f32[128]{0:T(128)S(1)} %add_convert_fusion.1, f32[16,64]{1,0:T(8,128)S(1)} %get-tuple-element.132), kind=kLoop, calls=%fused_computation.36 | loop fusion | flops 524288 | bytes 1057280 | tf_op jit(solution)/shard_map/mul | solution.py:109
  54.8 22.0 %all-gather = f32[128,64]{1,0:T(8,128)S(1)} all-gather(f32[64,64]{1,0:T(8,128)S(1)} %pad_maximum_fusion.1), channel_id=2, replica_groups=mesh['grp'=2,'sp_0'=16,'sp_1'=2,'tp'=4] {'sp_1'}, dimensions={0}, use_global_device_ids=true | all-gather | bytes 49152 | tf_op jit(solution)/shard_map/all_gather | solution.py:37
  76.8 27.8 %all-gather.1 = f32[1024,64]{1,0:T(8,128)S(1)} all-gather(f32[64,64]{1,0:T(8,128)S(1)} %pad_maximum_fusion.2), channel_id=3, replica_groups=mesh['grp'=2,'sp_0'=16,'sp_1'=2,'tp'=4] {'sp_0'}, dimensions={0}, use_global_device_ids=true | all-gather | bytes 278528 | tf_op jit(solution)/shard_map/all_gather | solution.py:37
  104.7 6.7 %multiply_add_fusion = (bf16[128,16,64]{2,1,0:T(8,128)(2,1)S(1)}, bf16[128,16,64]{2,1,0:T(8,128)(2,1)S(1)}) fusion(f32[128,16,64]{2,1,0:T(8,128)S(1)} %add.447, f32[16,64]{1,0:T(8,128)S(1)} %add_bitcast_fusion, f32[16,64]{1,0:T(8,128)S(1)} %get-tuple-element.108, f32[16,64]{1,0:T(8,128)S(1)} %get-tuple-element.133, f32[128]{0:T(128)S(1)} %add_convert_fusion.1, ...), kind=kLoop, calls=%fused_computation.42 | loop fusion | flops 1835008 | bytes 1589760 | tf_op jit(solution)/shard_map/add | solution.py:229
  111.4 0.4 fusion.25
  111.8 1.3 fusion.44
  113.1 0.2 convert_element_type.64
  113.3 0.8 copy.58
  114.1 3.8 %all-to-all-start = ((bf16[4,32,256]{2,1,0:T(8,128)(2,1)}), bf16[4,32,256]{2,1,0:T(8,128)(2,1)S(1)}, u32[]{:S(2)}, u32[]{:S(2)}) async-start(bf16[4,32,256]{2,1,0:T(8,128)(2,1)} %copy.58), calls=%async_computation | async-start | bytes 131072 | tf_op jit(solution)/shard_map/all_to_all | solution.py:233
  117.9 4.5 %all-to-all-done = bf16[4,32,256]{2,1,0:T(8,128)(2,1)S(1)} async-done(((bf16[4,32,256]{2,1,0:T(8,128)(2,1)}), bf16[4,32,256]{2,1,0:T(8,128)(2,1)S(1)}, u32[]{:S(2)}, u32[]{:S(2)}) %all-to-all-start) | async-done | bytes 65568 | tf_op jit(solution)/shard_map/all_to_all | solution.py:233
  122.4 3.6 %multiply_reduce_fusion = (f32[32]{0:T(128)S(1)}, f32[32,2048]{1,0:T(8,128)S(1)}) fusion(bf16[1024,2048]{1,0:T(8,128)(2,1)} %param.31, bf16[32,1024]{1,0:T(8,128)(2,1)S(1)} %bitcast.184, bf16[1024,1024]{1,0:T(8,128)(2,1)S(1)} %copy-done, f32[1024]{0:T(1024)S(1)} %copy-done.3, bf16[128,2048]{1,0:T(8,128)(2,1)} %param.20, s32[]{:T(128)S(6)} %select_n.296), kind=kOutput, calls=%fused_computation.57 | convolution fusion | flops 201818080 | bytes 6819972 | tf_op jit(solution)/shard_map/dot_general | solution.py:237
  126.2 0.9 broadcast_in_dim.32
  127.0 3.8 %all-to-all-start.1 = ((bf16[4,32,2048]{2,1,0:T(8,128)(2,1)}), bf16[4,32,2048]{2,1,0:T(8,128)(2,1)S(1)}, u32[]{:S(2)}, u32[]{:S(2)}) async-start(bf16[4,32,2048]{2,1,0:T(8,128)(2,1)} %broadcast_in_dim.32), calls=%async_computation.1 | async-start | bytes 1048576 | tf_op jit(solution)/shard_map/all_to_all | solution.py:63
  130.9 3.7 %copy.64 = bf16[8,8,32,1408]{3,2,1,0:T(8,128)(2,1)S(1)} copy(bf16[8,8,32,1408]{3,1,2,0:T(8,128)(2,1)} %bitcast.166) | data formatting | bytes 11534336
  134.6 4.5 %copy.60 = bf16[1408,32,64]{0,2,1:T(8,128)(2,1)} copy(bf16[1408,32,64]{0,1,2:T(8,128)(2,1)S(1)} %bitcast.165) | data formatting | bytes 11534336 | tf_op jit(solution)/shard_map/reshape | solution.py:246
  139.0 39.1 %all-gather.6.cloned.1.call-done = bf16[2048,2816]{1,0:T(8,128)(2,1)} async-done(((bf16[64,2816]{1,0:T(8,128)(2,1)}), bf16[2048,2816]{1,0:T(8,128)(2,1)}) %all-gather.6.cloned.1.call-update) | async-done | bytes 11534352 | tf_op jit(solution)/shard_map/all_gather | solution.py:20
  178.2 4.5 %fusion.2 = f32[128,1408]{1,0:T(8,128)} fusion(bf16[128,2048]{1,0:T(8,128)(2,1)S(1)} %bitcast.177, bf16[2048,2816]{1,0:T(8,128)(2,1)} %all-gather.6.cloned.1.call-done), kind=kOutput, calls=%fused_computation.10 | convolution fusion | flops 738197504 | bytes 7012352 | tf_op jit(solution)/shard_map/dot_general | solution.py:242
  182.7 7.4 %convolution_convert_fusion = bf16[128,2048]{1,0:T(8,128)(2,1)S(1)} fusion(bf16[1408,2048]{0,1:T(8,128)(2,1)} %bitcast.167, bf16[128,2048]{1,0:T(8,128)(2,1)S(1)} %bitcast.178, bf16[2048,2816]{1,0:T(8,128)(2,1)} %all-gather.6.cloned.1.call-done, f32[128,1408]{1,0:T(8,128)} %fusion.2), kind=kOutput, calls=%fused_computation.14 | convolution fusion | flops 1477738496 | bytes 13303808 | tf_op jit(solution)/shard_map/dot_general | solution.py:248
  190.1 12.8 %all_to_all.26 = bf16[4,32,2048]{2,1,0:T(8,128)(2,1)S(1)} all-to-all(bf16[4,32,2048]{2,1,0:T(8,128)(2,1)S(1)} %bitcast.179), channel_id=1, replica_groups=mesh['grp'=2,'sp_0'=16,'sp_1'=2,'tp'=4] {'tp'}, dimensions={0} | all-to-all | bytes 1048576 | tf_op jit(solution)/shard_map/all_to_all | solution.py:87
  202.9 0.7 add_convert_fusion
  (74 shorter events, 1.8 us)
Async XLA Ops:
  6.5 115.9 %copy-start = (bf16[1024,1024]{1,0:T(8,128)(2,1)S(1)}, bf16[1024,1024]{1,0:T(8,128)(2,1)}, u32[]{:S(2)}) copy-start(bf16[1024,1024]{1,0:T(8,128)(2,1)} %param.29) | copy-start | bytes 6291460
  6.6 124.3 %all-gather.8.cloned.1.call-start = ((), (), s32[]{:S(2)}) async-start(), calls=%async_computation.4 | async-start | bytes 5947392 | tf_op jit(solution)/shard_map/all_gather | solution.py:245
  7.3 170.8 %all-gather.6.cloned.1.call-start = ((), (), s32[]{:S(2)}) async-start(), calls=%async_computation.3 | async-start | bytes 11894784 | tf_op jit(solution)/shard_map/all_gather | solution.py:20
  25.7 24.4 %copy-start.4 = (f32[256]{0:T(256)S(1)}, f32[256]{0:T(256)}, u32[]{:S(2)}) copy-start(f32[256]{0:T(256)} %param.28) | copy-start | bytes 3076
  44.5 66.9 %copy-start.1 = (f32[16,16,64]{2,1,0:T(8,128)S(1)}, f32[16,16,64]{2,1,0:T(8,128)}, u32[]{:S(2)}) copy-start(f32[16,16,64]{2,1,0:T(8,128)} %param.26) | copy-start | bytes 196612
  47.8 74.7 %copy-start.3 = (f32[1024]{0:T(1024)S(1)}, f32[1024]{0:T(1024)}, u32[]{:S(2)}) copy-start(f32[1024]{0:T(1024)} %param.30) | copy-start | bytes 12292
  104.7 21.4 %copy-start.2 = (f32[2048]{0:T(1024)S(1)}, f32[2048]{0:T(1024)}, u32[]{:S(2)}) copy-start(f32[2048]{0:T(1024)} %param.32) | copy-start | bytes 24580
  114.1 8.3 %all-to-all-start = ((bf16[4,32,256]{2,1,0:T(8,128)(2,1)}), bf16[4,32,256]{2,1,0:T(8,128)(2,1)S(1)}, u32[]{:S(2)}, u32[]{:S(2)}) async-start(bf16[4,32,256]{2,1,0:T(8,128)(2,1)} %copy.58), calls=%async_computation | async-start | bytes 131072 | tf_op jit(solution)/shard_map/all_to_all | solution.py:233
  127.0 12.0 %all-to-all-start.1 = ((bf16[4,32,2048]{2,1,0:T(8,128)(2,1)}), bf16[4,32,2048]{2,1,0:T(8,128)(2,1)S(1)}, u32[]{:S(2)}, u32[]{:S(2)}) async-start(bf16[4,32,2048]{2,1,0:T(8,128)(2,1)} %broadcast_in_dim.32), calls=%async_computation.1 | async-start | bytes 1048576 | tf_op jit(solution)/shard_map/all_to_all | solution.py:63
Sparse Core Ops, SparseCore 0:
  9.2 89.1 all-gather.7
  100.2 77.8 all-gather.5
